TPU v7x, 32 devices: a whole 2x2x4 slice. The times are simulated.
32 devices in a mesh: sp: 8 (over z, x), tp: 4 (over y, core).
Axes of the slice: x: 2, y: 2, z: 4, core: 2. Of those that a mesh axis runs over, the one named last changes fastest.
Arguments:
- inputs: bfloat16 [8192, 2048], P('sp'), may hold values from -6 to 6
- w_query: bfloat16 [2048, 2048], P(None, 'tp'), may hold values from -0.125 to 0.125
- w_key: bfloat16 [2048, 2048], P(None, 'tp'), may hold values from -0.125 to 0.125
- w_value: bfloat16 [2048, 2048], P(None, 'tp'), may hold values from -0.125 to 0.125
- rel_table: float32 [16, 257], P('tp'), may hold values from -4 to 254
- out_grad: bfloat16 [8192, 2048], P('sp', 'tp'), may hold values from -6 to 6
Outputs:
- query_grad: bfloat16 [8192, 2048], P('sp', 'tp')
- key_grad: bfloat16 [8192, 2048], P('sp', 'tp')
- value_grad: bfloat16 [8192, 2048], P('sp', 'tp')
- query_weight_grad: float32 [2048, 2048], P('sp', 'tp')
- key_weight_grad: float32 [2048, 2048], P('sp', 'tp')
- value_weight_grad: float32 [2048, 2048], P('sp', 'tp')
- table_grad: float32 [16, 257], P('tp')
All inputs are finite; a program needn't handle non-finite values.
Results may differ from a plain program's by a relative error of at most 0.017.
The roundings to bfloat16 on the way count: a program that leaves them out, or rounds other values in their place, can miss the bound.
Values may be sent and summed in bfloat16 or wider, within the bound.
A program may use at most 128 MiB of HBM per device.

v0:
```python
import jax
import jax.numpy as jnp
from jax import lax
from jax.sharding import PartitionSpec as P

HDIM = 128
SEG = 64
PREV = 4
MAXREL = 128


def from_behind(block, axis, distance):
    devices = range(lax.axis_size(axis))
    route = [(i - distance, i) for i in devices if i - distance in devices]
    return lax.ppermute(block, axis, route)


def project(inputs, weight):
    return jnp.dot(inputs, weight, preferred_element_type=jnp.float32).astype(jnp.bfloat16)


def masked_scores(query_blk, key_blk, bias_band, query_pos, key_pos, score_scale):
    raw_scores = (
        jnp.einsum("qhd,khd->hqk", query_blk, key_blk, preferred_element_type=jnp.float32)
        * score_scale
    )
    seg_start = query_pos // SEG * SEG
    inside = (
        (key_pos[None, :] >= 0)
        & (key_pos[None, :] >= seg_start[:, None] - PREV * SEG)
        & (key_pos[None, :] < seg_start[:, None] + SEG)
    )
    return jnp.where(inside[None], raw_scores + bias_band, -jnp.inf)


def pair_grads(query_blk, grad_blk, key_blk, value_blk, probs_full, out_dot, score_scale):
    probs_low = probs_full.astype(jnp.bfloat16)
    value_part = jnp.einsum("hqk,qhd->khd", probs_low, grad_blk, preferred_element_type=jnp.float32)
    prob_grad = jnp.einsum("qhd,khd->hqk", grad_blk, value_blk, preferred_element_type=jnp.float32)
    score_grad = probs_full * (prob_grad - out_dot[:, :, None])
    score_low = score_grad.astype(jnp.bfloat16)
    key_part = score_scale * jnp.einsum(
        "hqk,qhd->khd", score_low, query_blk, preferred_element_type=jnp.float32
    )
    query_part = None
    query_part = score_scale * jnp.einsum(
        "hqk,khd->qhd", score_low, key_blk, preferred_element_type=jnp.float32
    )
    return (score_grad, query_part, key_part, value_part)


def diagonal_sums(matrix):
    head_count, row_count, col_count = matrix.shape
    widened = jnp.pad(matrix, ((0, 0), (0, 0), (row_count, 0)))
    flat = widened.reshape(head_count, row_count * (row_count + col_count))
    flat = jnp.pad(flat, ((0, 0), (0, row_count)))
    skewed = flat.reshape(head_count, row_count, row_count + col_count + 1)
    return jnp.sum(skewed, axis=1)


def bias_toeplitz(by_distance, reach):
    head_count = by_distance.shape[0]
    rolled = jnp.concatenate([by_distance[:, reach:], by_distance[:, :reach]], axis=1)
    tiled = jnp.tile(rolled, (1, reach))[:, : reach * 3 * reach]
    return tiled.reshape(head_count, reach, 3 * reach)[:, :, : 2 * reach]


def weight_term(inputs, grads):
    return jnp.einsum("td,tc->dc", inputs, grads, preferred_element_type=jnp.float32)


def local(inputs, w_query, w_key, w_value, rel_table, out_grad):
    row_count = inputs.shape[0]
    head_count = w_query.shape[1] // HDIM
    width = head_count * HDIM
    reach = PREV * SEG
    score_scale = HDIM ** (-0.5)
    offset = lax.axis_index("sp") * row_count
    diag_index = 2 * reach - jnp.arange(3 * reach + 1, dtype=jnp.int32)
    diag_bucket = jnp.clip(diag_index, -MAXREL, MAXREL) + MAXREL
    one_hot = (diag_bucket[:, None] == jnp.arange(2 * MAXREL + 1, dtype=jnp.int32)[None, :]).astype(
        jnp.float32
    )
    by_distance = jnp.einsum("hr,jr->hj", rel_table, one_hot, precision=lax.Precision.HIGHEST)
    bias_band = bias_toeplitz(by_distance, reach)
    query = project(inputs, w_query).reshape(row_count, head_count, HDIM)
    key_rows = project(inputs, w_key).reshape(row_count, head_count, HDIM)
    value_rows = project(inputs, w_value).reshape(row_count, head_count, HDIM)
    upstream = out_grad.reshape(row_count, head_count, HDIM)
    carried = from_behind(
        jnp.stack([key_rows[row_count - reach :], value_rows[row_count - reach :]]), "sp", 1
    )
    key_ext = jnp.concatenate([carried[0], key_rows], axis=0)
    value_ext = jnp.concatenate([carried[1], value_rows], axis=0)
    key_acc = jnp.zeros((row_count + reach, head_count, HDIM), jnp.float32)
    value_acc = jnp.zeros((row_count + reach, head_count, HDIM), jnp.float32)
    query_parts = []
    diag_total = jnp.zeros((head_count, 3 * reach + 1), jnp.float32)
    for block_idx in range(row_count // reach):
        first_row = block_idx * reach
        query_blk = query[first_row : first_row + reach]
        grad_blk = upstream[first_row : first_row + reach]
        key_blk = key_ext[first_row : first_row + 2 * reach]
        value_blk = value_ext[first_row : first_row + 2 * reach]
        query_pos = offset + first_row + jnp.arange(reach, dtype=jnp.int32)
        key_pos = offset + first_row - reach + jnp.arange(2 * reach, dtype=jnp.int32)
        scores = masked_scores(query_blk, key_blk, bias_band, query_pos, key_pos, score_scale)
        row_max = jnp.max(scores, axis=-1, keepdims=True)
        log_norm = row_max[:, :, 0] + jnp.log(jnp.sum(jnp.exp(scores - row_max), axis=-1))
        probs_full = jnp.exp(scores - log_norm[:, :, None])
        attn_out = jnp.einsum(
            "hqk,khd->qhd",
            probs_full.astype(jnp.bfloat16),
            value_blk,
            preferred_element_type=jnp.float32,
        ).astype(jnp.bfloat16)
        out_dot = jnp.einsum("qhd,qhd->hq", grad_blk, attn_out, preferred_element_type=jnp.float32)
        score_grad, query_part, key_part, value_part = pair_grads(
            query_blk, grad_blk, key_blk, value_blk, probs_full, out_dot, score_scale
        )
        query_parts.append(query_part)
        key_acc = key_acc.at[first_row : first_row + 2 * reach].add(key_part)
        value_acc = value_acc.at[first_row : first_row + 2 * reach].add(value_part)
        diag_total = diag_total + diagonal_sums(score_grad)
    query_grad = jnp.concatenate(query_parts, axis=0).astype(jnp.bfloat16).reshape(row_count, width)
    returned = from_behind(jnp.stack([key_acc[:reach], value_acc[:reach]]), "sp", -1)
    key_own = key_acc[reach:].at[row_count - reach :].add(returned[0])
    value_own = value_acc[reach:].at[row_count - reach :].add(returned[1])
    key_grad = key_own.astype(jnp.bfloat16).reshape(row_count, width)
    value_grad = value_own.astype(jnp.bfloat16).reshape(row_count, width)
    all_sums = lax.psum_scatter(
        weight_term(inputs, jnp.concatenate([query_grad, key_grad, value_grad], axis=1)),
        "sp",
        scatter_dimension=0,
        tiled=True,
    )
    query_weight_grad = all_sums[:, :width]
    key_weight_grad = all_sums[:, width : 2 * width]
    value_weight_grad = all_sums[:, 2 * width :]
    table_local = jnp.dot(diag_total, one_hot, precision=lax.Precision.HIGHEST)
    table_grad = lax.psum(table_local, "sp")
    return (
        query_grad,
        key_grad,
        value_grad,
        query_weight_grad,
        key_weight_grad,
        value_weight_grad,
        table_grad,
    )


def solution(mesh):
    placed = (
        P("sp", None),
        P(None, "tp"),
        P(None, "tp"),
        P(None, "tp"),
        P("tp", None),
        P("sp", "tp"),
    )
    return jax.shard_map(
        local,
        mesh=mesh,
        in_specs=placed,
        out_specs=(
            P("sp", "tp"),
            P("sp", "tp"),
            P("sp", "tp"),
            P("sp", "tp"),
            P("sp", "tp"),
            P("sp", "tp"),
            P("tp", None),
        ),
        check_vma=False,
    )
```

profile of v0, /device:TPU:0, one launch (start us, length us, event | category | flops | bytes accessed | tf_op | source)
XLA Modules:
  0.0 350.6 jit_solution(6757611684122161515)
XLA Ops:
  7.2 1.5 copy-done
  8.8 4.6 %convolution_convert_fusion.2 = bf16[1024,512]{0,1:T(8,128)(2,1)S(1)} fusion(bf16[1024,2048]{1,0:T(8,128)(2,1)} %param.26, bf16[2048,512]{1,0:T(8,128)(2,1)S(1)} %copy-done), kind=kOutput, calls=%fused_computation.39 | convolution fusion | flops 2148007936 | bytes 7340032 | tf_op jit(solution)/shard_map/dot_general | solution.py:19
  13.6 5.4 %convolution_convert_fusion.1 = bf16[1024,512]{0,1:T(8,128)(2,1)S(1)} fusion(bf16[1024,2048]{1,0:T(8,128)(2,1)} %param.26, bf16[2048,512]{1,0:T(8,128)(2,1)} %param.29), kind=kOutput, calls=%fused_computation.38 | convolution fusion | flops 2148007936 | bytes 7340032 | tf_op jit(solution)/shard_map/dot_general | solution.py:19
  20.0 5.7 %collective-permute-start = (bf16[2,256,4,128]{3,1,2,0:T(8,128)(2,1)}, bf16[2,256,4,128]{3,1,2,0:T(8,128)(2,1)}, u32[]{:S(2)}, u32[]{:S(2)}) collective-permute-start(bf16[2,256,4,128]{3,1,2,0:T(8,128)(2,1)} %pad_maximum_fusion.4), channel_id=1, source_target_pairs={{0,4},{4,8},{8,12},{12,16},{16,20},{20,24},{24,28},{1,5},{5,9},{9,... | collective-permute-start | bytes 1572872 | tf_op jit(solution)/shard_map/ppermute | solution.py:15
  26.6 1.3 fusion.85
  27.8 1.2 fusion.86
  29.0 1.3 copy.51
  31.2 5.2 %convolution_convert_fusion = bf16[1024,512]{0,1:T(8,128)(2,1)S(1)} fusion(bf16[1024,2048]{1,0:T(8,128)(2,1)} %param.26, bf16[2048,512]{1,0:T(8,128)(2,1)} %param.27), kind=kOutput, calls=%fused_computation.37 | convolution fusion | flops 2148007936 | bytes 7340032 | tf_op jit(solution)/shard_map/dot_general | solution.py:19
  38.6 1.1 copy.132
  41.7 1.9 copy.135
  43.7 2.0 tile.4
  45.7 6.9 %tile.10 = f32[4,196864]{1,0:T(4,128)} reshape(f32[4,256,769]{2,1,0:T(8,128)} %tile.4) | data formatting | bytes 6299648 | tf_op jit(solution)/shard_map/tile | solution.py:64
  52.6 1.9 slice-done
  61.6 1.9 bitcast_multiply_fusion.2
  67.0 1.5 slice_bitcast_fusion.4
  80.2 1.2 pad_maximum_fusion.1
  81.4 1.3 collective-permute-start.1
  84.1 2.2 fusion.31
  87.2 2.2 fusion.32
  90.3 2.9 slice.456
  93.2 2.7 slice.463
  97.2 11.0 %collective-permute-done.1 = f32[2,256,4,128]{1,3,2,0:T(8,128)} collective-permute-done((f32[2,256,4,128]{1,3,2,0:T(8,128)}, f32[2,256,4,128]{1,3,2,0:T(8,128)}, u32[]{:S(2)}, u32[]{:S(2)}) %collective-permute-start.1) | collective-permute-done | bytes 1048608 | tf_op jit(solution)/shard_map/ppermute | solution.py:15
  108.2 2.4 fusion.55
  110.7 2.7 copy.81
  113.3 1.3 copy.80
  114.6 12.0 %convolution_bitcast_fusion = f32[2048,1536]{0,1:T(8,128)} fusion(bf16[1024,2048]{1,0:T(8,128)(2,1)} %param.26, bf16[1024,512]{1,0:T(8,128)(2,1)} %copy.81, bf16[1024,512]{1,0:T(8,128)(2,1)} %copy.80, bf16[256,512]{1,0:T(8,128)(2,1)} %copy.77, bf16[256,512]{1,0:T(8,128)(2,1)} %copy.76, bf16[256,512]{1,0:T(8,128)(2,1)S(1)} %copy-done.35, bf16[256,512]{1,0:T(8,128)(2,1)} %copy.74), kind=kOutput, calls=%fused_computation | convolution fusion | flops 6461325312 | bytes 19922944 | tf_op jit(solution)/shard_map/td,tc->dc/dot_general | solution.py:69
  126.7 1.9 pad_bitcast_fusion
  128.6 2.0 copy.140
  130.6 2.4 pad.55
  133.0 8.4 %reshape.842 = f32[4,256,769]{2,1,0:T(8,128)} reshape(f32[4,196864]{1,0:T(4,128)} %pad.55) | data formatting | bytes 6299648 | tf_op jit(solution)/shard_map/reshape | solution.py:57
  141.4 2.2 reduce_sum.79
  143.6 1.9 pad_bitcast_fusion.1
  145.5 2.0 copy.139
  147.5 2.1 pad.53
  149.7 7.8 %reshape.840 = f32[4,256,769]{2,1,0:T(8,128)} reshape(f32[4,196864]{1,0:T(4,128)} %pad.53) | data formatting | bytes 6299648 | tf_op jit(solution)/shard_map/reshape | solution.py:57
  157.5 2.2 reduce_sum.78
  160.0 2.0 copy.138
  162.0 2.1 pad.51
  164.2 7.9 %reshape.838 = f32[4,256,769]{2,1,0:T(8,128)} reshape(f32[4,196864]{1,0:T(4,128)} %pad.51) | data formatting | bytes 6299648 | tf_op jit(solution)/shard_map/reshape | solution.py:57
  172.1 2.4 reduce_sum.77
  175.1 2.0 copy.137
  177.2 2.0 pad.49
  179.2 7.8 %reshape.836 = f32[4,256,769]{2,1,0:T(8,128)} reshape(f32[4,196864]{1,0:T(4,128)} %pad.49) | data formatting | bytes 6299648 | tf_op jit(solution)/shard_map/reshape | solution.py:57
  187.0 2.3 reduce_sum.76
  189.9 21.2 %psum.7 = f32[4,257]{1,0:T(4,128)} all-reduce(f32[4,257]{1,0:T(4,128)S(1)} %fusion.33), channel_id=1, replica_groups=mesh['sp'=8,'tp'=4] {'sp'}, use_global_device_ids=true, to_apply=%region_13.14 | all-reduce | flops 1028 | bytes 8224 | tf_op jit(solution)/shard_map/psum | solution.py:141
  212.1 124.9 %reduce-scatter.2.cloned.1.call-done = f32[256,1536]{0,1:T(8,128)} async-done(((f32[2048,1536]{0,1:T(8,128)}), f32[256,1536]{0,1:T(8,128)}) %reduce-scatter.2.cloned.1.call-update) | async-done | bytes 1572880 | tf_op jit(solution)/shard_map/reduce_scatter | solution.py:131
  337.1 2.4 fusion.82
  339.5 2.0 copy.84
  (163 shorter events, 37.9 us)
Async XLA Ops:
  7.2 1.6 copy-start
  7.2 329.9 %reduce-scatter.2.cloned.1.call-start = ((), (), s32[]{:S(2)}) async-start(), calls=%async_computation.1 | async-start | bytes 14155776 | tf_op jit(solution)/shard_map/reduce_scatter | solution.py:131
  13.3 14.5 %copy-start.10 = (bf16[1024,512]{0,1:T(8,128)(2,1)}, bf16[1024,512]{0,1:T(8,128)(2,1)S(1)}, u32[]{:S(2)}) copy-start(bf16[1024,512]{0,1:T(8,128)(2,1)S(1)} %convolution_convert_fusion.2) | copy-start | bytes 3145732
  18.9 6.9 %copy-start.40 = (f32[4,257]{1,0:T(4,128)S(1)}, f32[4,257]{1,0:T(4,128)}, u32[]{:S(2)}) copy-start(f32[4,257]{1,0:T(4,128)} %param.30) | copy-start | bytes 12340
  20.0 47.0 %collective-permute-start = (bf16[2,256,4,128]{3,1,2,0:T(8,128)(2,1)}, bf16[2,256,4,128]{3,1,2,0:T(8,128)(2,1)}, u32[]{:S(2)}, u32[]{:S(2)}) collective-permute-start(bf16[2,256,4,128]{3,1,2,0:T(8,128)(2,1)} %pad_maximum_fusion.4), channel_id=1, source_target_pairs={{0,4},{4,8},{8,12},{12,16},{16,20},{20,24},{24,28},{1,5},{5,9},{9,... | collective-permute-start | bytes 1572872 | tf_op jit(solution)/shard_map/ppermute | solution.py:15
  26.6 2.5 copy-start.39
  29.0 1.3 copy-start.11
  36.4 1.3 copy-start.34
  37.7 17.6 %copy-start.31 = (bf16[256,512]{0,1:T(8,128)(2,1)}, bf16[256,512]{0,1:T(8,128)(2,1)S(1)}, u32[]{:S(2)}) copy-start(bf16[256,512]{0,1:T(8,128)(2,1)S(1)} %get-tuple-element.153) | copy-start | bytes 786436
  37.7 19.5 %copy-start.29 = (bf16[256,512]{0,1:T(8,128)(2,1)}, bf16[256,512]{0,1:T(8,128)(2,1)S(1)}, u32[]{:S(2)}) copy-start(bf16[256,512]{0,1:T(8,128)(2,1)S(1)} %get-tuple-element.152) | copy-start | bytes 786436
  37.7 21.2 %copy-start.27 = (bf16[256,512]{0,1:T(8,128)(2,1)}, bf16[256,512]{0,1:T(8,128)(2,1)S(1)}, u32[]{:S(2)}) copy-start(bf16[256,512]{0,1:T(8,128)(2,1)S(1)} %get-tuple-element.151) | copy-start | bytes 786436
  37.7 5.9 %slice-start.1 = ((f32[4,769]{1,0:T(4,128)}), f32[4,256]{1,0:T(4,128)S(1)}, s32[]{:S(2)}) async-start(f32[4,769]{1,0:T(4,128)} %copy-done.39), calls=%async_computation.3 | async-start | bytes 8192 | tf_op jit(solution)/shard_map/slice | solution.py:63
  37.7 5.8 %slice-start.2 = ((f32[4,769]{1,0:T(4,128)}), f32[4,513]{1,0:T(4,128)S(1)}, s32[]{:S(2)}) async-start(f32[4,769]{1,0:T(4,128)} %copy-done.39), calls=%async_computation.4 | async-start | bytes 20480 | tf_op jit(solution)/shard_map/slice | solution.py:63
  41.7 18.8 %copy-start.23 = (bf16[256,512]{0,1:T(8,128)(2,1)}, bf16[256,512]{0,1:T(8,128)(2,1)S(1)}, u32[]{:S(2)}) copy-start(bf16[256,512]{0,1:T(8,128)(2,1)S(1)} %copy.133) | copy-start | bytes 786436
  52.6 1.9 slice-start
  54.5 1.0 copy-start.16
  56.3 1.0 copy-start.15
  58.0 1.0 copy-start.14
  59.8 1.0 copy-start.19
  61.5 1.9 copy-start.18
  61.6 1.9 copy-start.21
  64.1 1.0 copy-start.17
  64.1 1.1 copy-start.22
  65.0 9.5 %copy-start.2 = (f32[4,256,512]{2,1,0:T(8,128)}, f32[4,256,512]{2,1,0:T(8,128)S(1)}, u32[]{:S(2)}) copy-start(f32[4,256,512]{2,1,0:T(8,128)S(1)} %bitcast_multiply_fusion.1) | copy-start | bytes 6291460
  66.1 2.3 copy-start.33
  67.0 8.5 %copy-start.3 = (f32[4,256,512]{2,1,0:T(8,128)}, f32[4,256,512]{2,1,0:T(8,128)S(1)}, u32[]{:S(2)}) copy-start(f32[4,256,512]{2,1,0:T(8,128)S(1)} %bitcast_multiply_fusion) | copy-start | bytes 6291460
  68.5 0.8 copy-start.25
  69.9 1.2 copy-start.9
  72.7 1.3 copy-start.4
  73.0 1.1 copy-start.32
  74.2 0.9 copy-start.30
  75.1 0.9 copy-start.28
  76.4 1.0 copy-start.12
  76.5 1.7 copy-start.8
  76.5 1.7 copy-start.24
  80.1 1.3 copy-start.13
  80.2 3.0 copy-start.7
  81.4 26.8 %collective-permute-start.1 = (f32[2,256,4,128]{1,3,2,0:T(8,128)}, f32[2,256,4,128]{1,3,2,0:T(8,128)}, u32[]{:S(2)}, u32[]{:S(2)}) collective-permute-start(f32[2,256,4,128]{1,3,2,0:T(8,128)} %pad_maximum_fusion.1), channel_id=1, source_target_pairs={{4,0},{8,4},{12,8},{16,12},{20,16},{24,20},{28,24},{5,1},{9,5},{13... | collective-permute-start | bytes 3145736 | tf_op jit(solution)/shard_map/ppermute | solution.py:15
  90.3 5.6 %copy-start.5 = (f32[4,256,512]{2,1,0:T(8,128)S(1)}, f32[4,256,512]{2,1,0:T(8,128)}, u32[]{:S(2)}) copy-start(f32[4,256,512]{2,1,0:T(8,128)} %copy-done.4) | copy-start | bytes 6291460
  90.3 5.6 %copy-start.26 = (bf16[256,4,128]{2,0,1:T(8,128)(2,1)S(1)}, bf16[256,4,128]{2,0,1:T(8,128)(2,1)}, u32[]{:S(2)}) copy-start(bf16[256,4,128]{2,0,1:T(8,128)(2,1)} %copy-done.25) | copy-start | bytes 786436
  110.7 2.7 copy-start.20
  110.7 4.0 %copy-start.35 = (bf16[256,512]{1,0:T(8,128)(2,1)S(1)}, bf16[256,512]{1,0:T(8,128)(2,1)}, u32[]{:S(2)}) copy-start(bf16[256,512]{1,0:T(8,128)(2,1)} %copy.75) | copy-start | bytes 786436
  172.1 2.8 copy-start.6
  187.0 24.1 %copy-start.36 = (bf16[256,512]{1,0:T(8,128)(2,1)S(1)}, bf16[256,512]{1,0:T(8,128)(2,1)}, u32[]{:S(2)}) copy-start(bf16[256,512]{1,0:T(8,128)(2,1)} %copy.76) | copy-start | bytes 786436
  187.0 24.1 %copy-start.37 = (bf16[256,512]{1,0:T(8,128)(2,1)S(1)}, bf16[256,512]{1,0:T(8,128)(2,1)}, u32[]{:S(2)}) copy-start(bf16[256,512]{1,0:T(8,128)(2,1)} %copy.77) | copy-start | bytes 786436
  187.0 24.1 %copy-start.38 = (bf16[256,512]{1,0:T(8,128)(2,1)S(1)}, bf16[256,512]{1,0:T(8,128)(2,1)}, u32[]{:S(2)}) copy-start(bf16[256,512]{1,0:T(8,128)(2,1)} %copy.74) | copy-start | bytes 786436
  337.1 6.4 %copy-start.1 = (bf16[2048,512]{1,0:T(8,128)(2,1)S(1)}, bf16[2048,512]{1,0:T(8,128)(2,1)}, u32[]{:S(2)}) copy-start(bf16[2048,512]{1,0:T(8,128)(2,1)} %param.28) | copy-start | bytes 6291460
Sparse Core Ops, SparseCore 0:
  126.8 210.2 reduce-scatter.1
where the time goes:
time: 357 us; the launch traced here: 351 us
  waiting for transfers between devices  136 us (38%)
  local copies, waits for them, and re-layouts  105 us (29%)
  matrix products  47.6 us (13%)
  blocking collectives  21.2 us (6%)
  other arithmetic  18.5 us (5%)
  between operations  15.1 us (4%)
  starting transfers between devices  6.98 us (2%)
    reduce_scatter x1, waiting for transfers between devices, local(): lax.psum_scatter(weight_term(inputs, jnp.concatenate([query_grad, key_gra...  125 us
    unnamed x100, local copies, waits for them, and re-layouts  33.6 us
    reshape x4, local copies, waits for them, and re-layouts, diagonal_sums(): skewed = flat.reshape(head_count, row_count, row_count + col_count + 1)  32 us
    psum x1, blocking collectives, local(): table_grad = lax.psum(table_local, 'sp')  21.2 us
    dot_general x3, matrix products, project(): jnp.dot(inputs, weight, preferred_element_type=jnp.float32)  15.2 us
    dot_general x1, matrix products, weight_term(): jnp.einsum('td,tc->dc', inputs, grads, preferred_element_type=jnp.float32)  12 us
    ppermute x2, waiting for transfers between devices, from_behind(): return lax.ppermute(block, axis, route)  11 us
    reduce_sum x4, other arithmetic, diagonal_sums(): return jnp.sum(skewed, axis=1)  9.23 us
  transfers between devices with their start and end apart: 3, of which 2 were waited for; matrix products, arithmetic and copies ran while one was open for 33% of the time, Pallas kernels for 0%

commit v1 on v0

v1 whole, which is shorter than its diff:
```python
import functools

import jax
import jax.numpy as jnp
from jax import lax
from jax.experimental import pallas as pl
from jax.experimental.pallas import tpu as pltpu
from jax.sharding import PartitionSpec as P

HDIM = 128
SEG = 64
PREV = 4
MAXREL = 128
REACH = PREV * SEG
TILE = 2 * SEG
BAND = REACH + TILE
WRAP = 4 * MAXREL
GROUPS = 2


def from_behind(block, axis, distance):
    devices = range(lax.axis_size(axis))
    route = [(i - distance, i) for i in devices if i - distance in devices]
    return lax.ppermute(block, axis, route)


def project(inputs, weight):
    return jnp.dot(inputs, weight, preferred_element_type=jnp.float32).astype(jnp.bfloat16)


def contract(a, b, dims):
    return lax.dot_general(a, b, (dims, ((), ())), preferred_element_type=jnp.float32)


def attention_kernel(
    first_ref, bias_ref, q_ref, k_ref, v_ref, g_ref, hk_ref, hv_ref,
    dq_ref, dk_ref, dv_ref, hdk_ref, hdv_ref, tk_ref, tv_ref, diag_ref,
    kx, vx, dk_acc, dv_acc, band_acc,
):
    rows = q_ref.shape[0]
    scale = HDIM ** (-0.5)
    kx[:REACH] = hk_ref[...]
    kx[REACH:] = k_ref[...]
    vx[:REACH] = hv_ref[...]
    vx[REACH:] = v_ref[...]
    dk_acc[...] = jnp.zeros_like(dk_acc)
    dv_acc[...] = jnp.zeros_like(dv_acc)
    band_acc[...] = jnp.zeros_like(band_acc)
    row = lax.broadcasted_iota(jnp.int32, (TILE, BAND), 0)
    col = lax.broadcasted_iota(jnp.int32, (TILE, BAND), 1)
    start = row // SEG * SEG
    seen = (col >= start) & (col < start + REACH + SEG)
    wide = jnp.broadcast_to(bias_ref[0], (TILE, WRAP))
    bias = pltpu.roll(wide, 0, 1, stride=1, stride_axis=0)[:, :BAND]
    bias = jnp.where(seen, bias, -jnp.inf)
    is_first = first_ref[0] == 0
    for blk in range(rows // TILE):
        lo = blk * TILE
        q = q_ref[lo : lo + TILE]
        g = g_ref[lo : lo + TILE]
        k = kx[lo : lo + BAND]
        v = vx[lo : lo + BAND]
        s = contract(q, k, ((1,), (1,))) * scale + bias
        if lo < REACH:
            s = jnp.where(is_first & (col < REACH - lo), -jnp.inf, s)
        m = jnp.max(s, axis=1, keepdims=True)
        e = jnp.exp(s - m)
        p = e * (1.0 / jnp.sum(e, axis=1, keepdims=True))
        p_low = p.astype(jnp.bfloat16)
        out = contract(p_low, v, ((1,), (0,))).astype(jnp.bfloat16)
        out_dot = jnp.sum(g.astype(jnp.float32) * out.astype(jnp.float32), axis=1, keepdims=True)
        dp = contract(g, v, ((1,), (1,)))
        ds = p * (dp - out_dot)
        ds_low = ds.astype(jnp.bfloat16)
        band_acc[:, :BAND] += ds
        dq_ref[lo : lo + TILE] = (contract(ds_low, k, ((1,), (0,))) * scale).astype(jnp.bfloat16)
        dk_acc[lo : lo + BAND] += contract(ds_low, q, ((0,), (0,)))
        dv_acc[lo : lo + BAND] += contract(p_low, g, ((0,), (0,)))
    dk_ref[...] = (dk_acc[REACH:] * scale).astype(jnp.bfloat16)
    dv_ref[...] = dv_acc[REACH:].astype(jnp.bfloat16)
    hdk_ref[...] = (dk_acc[:REACH] * scale).astype(jnp.bfloat16)
    hdv_ref[...] = dv_acc[:REACH].astype(jnp.bfloat16)
    tk_ref[...] = dk_acc[rows:] * scale
    tv_ref[...] = dv_acc[rows:]
    total = band_acc[...]
    half = TILE // 2
    while half >= 1:
        total = total[:half] + pltpu.roll(total[half:], WRAP - half, 1)
        half //= 2
    diag_ref[0] = total


def attention(first, bias_rows, query, keys, values, upstream, halo_k, halo_v, head0, heads):
    rows = query.shape[0]
    whole = pl.BlockSpec((rows, HDIM), lambda h: (0, h))
    shifted = pl.BlockSpec((rows, HDIM), lambda h: (0, head0 + h))
    edge = pl.BlockSpec((REACH, HDIM), lambda h: (0, h))
    line = pl.BlockSpec((1, 1, WRAP), lambda h: (head0 + h, 0, 0))
    width = heads * HDIM
    sds = jax.ShapeDtypeStruct
    flops = 12 * heads * rows * BAND * HDIM
    return pl.pallas_call(
        attention_kernel,
        grid=(heads,),
        in_specs=[pl.BlockSpec(memory_space=pltpu.SMEM), line, shifted, shifted, shifted, shifted,
                  pl.BlockSpec((REACH, HDIM), lambda h: (0, h)), pl.BlockSpec((REACH, HDIM), lambda h: (0, h))],
        out_specs=[whole, whole, whole, edge, edge, edge, edge,
                   pl.BlockSpec((1, 1, WRAP), lambda h: (h, 0, 0))],
        out_shape=[
            sds((rows, width), jnp.bfloat16), sds((rows, width), jnp.bfloat16), sds((rows, width), jnp.bfloat16),
            sds((REACH, width), jnp.bfloat16), sds((REACH, width), jnp.bfloat16),
            sds((REACH, width), jnp.float32), sds((REACH, width), jnp.float32),
            sds((heads, 1, WRAP), jnp.float32),
        ],
        scratch_shapes=[
            pltpu.VMEM((rows + REACH, HDIM), jnp.bfloat16), pltpu.VMEM((rows + REACH, HDIM), jnp.bfloat16),
            pltpu.VMEM((rows + REACH, HDIM), jnp.float32), pltpu.VMEM((rows + REACH, HDIM), jnp.float32),
            pltpu.VMEM((TILE, WRAP), jnp.float32),
        ],
        cost_estimate=pl.CostEstimate(flops=flops * 2, bytes_accessed=heads * rows * HDIM * 20, transcendentals=heads * rows * BAND),
    )(first, bias_rows, query, keys, values, upstream, halo_k, halo_v)


def local(inputs, w_query, w_key, w_value, rel_table, out_grad):
    rows = inputs.shape[0]
    head_count = w_query.shape[1] // HDIM
    first = lax.axis_index("sp").reshape(1)
    far = rel_table[:, 2 * MAXREL :]
    pad = jnp.broadcast_to(far, (head_count, MAXREL))
    bias_rows = jnp.concatenate([pad, rel_table[:, :0:-1], pad], axis=1)[:, None, :]
    keys = project(inputs, w_key)
    values = project(inputs, w_value)
    halo = from_behind(jnp.concatenate([keys[rows - REACH :], values[rows - REACH :]], axis=1), "sp", 1)
    query = project(inputs, w_query)
    width = head_count * HDIM
    heads = head_count // GROUPS
    span = heads * HDIM
    grads, sums, diags = [], [], []
    for group in range(GROUPS):
        at = group * span
        dq, dk, dv, hdk, hdv, tk, tv, diag = attention(
            first, bias_rows, query, keys, values, out_grad,
            halo[:, at : at + span], halo[:, width + at : width + at + span], group * heads, heads)
        back = from_behind(jnp.concatenate([hdk, hdv], axis=1), "sp", -1).astype(jnp.float32)
        dk = lax.dynamic_update_slice(dk, (tk + back[:, :span]).astype(jnp.bfloat16), (rows - REACH, 0))
        dv = lax.dynamic_update_slice(dv, (tv + back[:, span:]).astype(jnp.bfloat16), (rows - REACH, 0))
        part = jnp.einsum("td,tc->dc", inputs, jnp.concatenate([dq, dk, dv], axis=1),
                          preferred_element_type=jnp.float32).astype(jnp.bfloat16)
        sums.append(lax.psum_scatter(part, "sp", scatter_dimension=0, tiled=True))
        grads.append((dq, dk, dv))
        diags.append(diag)
    query_grad, key_grad, value_grad = [jnp.concatenate(parts, axis=1) for parts in zip(*grads)]
    wq, wk, wv = [
        jnp.concatenate([s[:, i * span : (i + 1) * span] for s in sums], axis=1).astype(jnp.float32)
        for i in range(3)
    ]
    diag = lax.psum(jnp.concatenate(diags, axis=0)[:, 0, :], "sp")
    top = jnp.sum(diag[:, : MAXREL + 1], axis=1, keepdims=True) + jnp.sum(diag[:, 3 * MAXREL :], axis=1, keepdims=True)
    table_grad = jnp.concatenate(
        [jnp.zeros((head_count, 1), jnp.float32), diag[:, MAXREL + 1 : 3 * MAXREL][:, ::-1], top], axis=1)
    return query_grad, key_grad, value_grad, wq, wk, wv, table_grad


def solution(mesh):
    placed = (
        P("sp", None),
        P(None, "tp"),
        P(None, "tp"),
        P(None, "tp"),
        P("tp", None),
        P("sp", "tp"),
    )
    return jax.shard_map(
        local,
        mesh=mesh,
        in_specs=placed,
        out_specs=(
            P("sp", "tp"),
            P("sp", "tp"),
            P("sp", "tp"),
            P("sp", "tp"),
            P("sp", "tp"),
            P("sp", "tp"),
            P("tp", None),
        ),
        check_vma=False,
    )
```

time: 357 us -> 239 us (0.67); the launches traced: 351 us -> 238 us
  local copies, waits for them, and re-layouts: 105 us -> 10.4 us
  Pallas kernels: 0 us -> 27.1 us
  waiting for transfers between devices: 136 us -> 109 us
  matrix products: 47.6 us -> 28.5 us
  blocking collectives: 21.2 us -> 31.4 us
  other arithmetic: 18.5 us -> 10.3 us
    reduce_scatter x1 -> x2, waiting for transfers between devices: 125 us -> 87.9 us  [local(): sums.append(lax.psum_scatter(part, 'sp', scatter_dimension=0, tiled=True))]
    reshape x6 -> x0, local copies, waits for them, and re-layouts: 34.1 us -> none  [the longest x4 32 us: diagonal_sums(): skewed = flat.reshape(head_count, row_count, row_count + col_count + 1)]
    unnamed x100 -> x34, local copies, waits for them, and re-layouts: 33.6 us -> 5.58 us
    pallas_call x0 -> x2, Pallas kernels: none -> 27.1 us  [attention(): pl.pallas_call(attention_kernel, grid=(heads,), in_specs=[pl.BlockSpec(me...]
    dot_general x27 -> x2, matrix products: 32.4 us -> 15.3 us  [local(): jnp.einsum('td,tc->dc', inputs, jnp.concatenate([dq, dk, dv], axis=1), pr...]
    reduce_sum x8 -> x2, other arithmetic: 11.9 us -> 0.23 us  [the longest x1 0.12 us: local(): jnp.sum(diag[:, :MAXREL + 1], axis=1, keepdims=True)]
    slice x15 -> x8, local copies, waits for them, and re-layouts: 14.1 us -> 3.87 us  [the longest x2 2.77 us: local(): s[:, i * span:(i + 1) * span]]
    psum x1, blocking collectives: 21.2 us -> 31.4 us  [local(): diag = lax.psum(jnp.concatenate(diags, axis=0)[:, 0, :], 'sp')]
  transfers between devices with their start and end apart: 3 -> 5, of which waited for: 2 -> 5; matrix products, arithmetic and copies ran while one was open for 33% -> 10% of each run, Pallas kernels for 0% -> 6%
where the time goes in v1:
time: 239 us; the launch traced here: 238 us
  waiting for transfers between devices  109 us (46%)
  blocking collectives  31.4 us (13%)
  matrix products  28.5 us (12%)
  Pallas kernels  27.1 us (11%)
  between operations  14.3 us (6%)
  local copies, waits for them, and re-layouts  10.4 us (4%)
  other arithmetic  10.3 us (4%)
  starting transfers between devices  7.75 us (3%)
    reduce_scatter x2, waiting for transfers between devices, local(): sums.append(lax.psum_scatter(part, 'sp', scatter_dimension=0, tiled=True))  87.9 us
    psum x1, blocking collectives, local(): diag = lax.psum(jnp.concatenate(diags, axis=0)[:, 0, :], 'sp')  31.4 us
    pallas_call x2, Pallas kernels, attention(): pl.pallas_call(attention_kernel, grid=(heads,), in_specs=[pl.BlockSpec(me...  27.1 us
    ppermute x3, waiting for transfers between devices, from_behind(): return lax.ppermute(block, axis, route)  20.7 us
    dot_general x2, matrix products, local(): jnp.einsum('td,tc->dc', inputs, jnp.concatenate([dq, dk, dv], axis=1), pr...  15.3 us
    dot_general x3, matrix products, project(): jnp.dot(inputs, weight, preferred_element_type=jnp.float32)  13.2 us
    ppermute x3, starting transfers between devices, from_behind(): return lax.ppermute(block, axis, route)  7.49 us
    unnamed x34, local copies, waits for them, and re-layouts  5.58 us
  transfers between devices with their start and end apart: 5, of which 5 were waited for; matrix products, arithmetic and copies ran while one was open for 10% of the time, Pallas kernels for 6%

profile of v1, /device:TPU:0, one launch (start us, length us, event | category | flops | bytes accessed | tf_op | source)
XLA Modules:
  0.0 238.5 jit_solution(18077501340604598850)
XLA Ops:
  7.2 1.5 copy-done
  8.8 4.7 %convolution_convert_fusion.3.k_ref = bf16[1024,512]{1,0:T(8,128)(2,1)S(1)} fusion(bf16[1024,2048]{1,0:T(8,128)(2,1)} %param.6, bf16[2048,512]{1,0:T(8,128)(2,1)S(1)} %copy-done), kind=kOutput, calls=%fused_computation.15 | convolution fusion | flops 2148007936 | bytes 7340032 | tf_op jit(solution)/shard_map/dot_general | solution.py:28
  13.5 2.3 convolution_convert_fusion.2.v_ref
  15.9 0.1 pad_maximum_fusion.3
  15.9 4.9 %collective-permute-start = (bf16[256,1024]{1,0:T(8,128)(2,1)S(1)}, bf16[256,1024]{1,0:T(8,128)(2,1)S(1)}, u32[]{:S(2)}, u32[]{:S(2)}) collective-permute-start(bf16[256,1024]{1,0:T(8,128)(2,1)S(1)} %pad_maximum_fusion.3), channel_id=1, source_target_pairs={{0,4},{4,8},{8,12},{12,16},{16,20},{20,24},{24,28},{1,5},{5,9},{9,... | collective-permute-start | bytes 1572872 | tf_op jit(solution)/shard_map/ppermute | solution.py:24
  20.9 0.1 slice.64
  20.9 0.1 slice_reduce_fusion.2
  21.1 0.2 rev.6
  21.3 0.1 broadcast_in_dim.13
  21.3 0.6 broadcast_in_dim.14.bias_ref
  21.9 6.2 %convolution_convert_fusion.4.q_ref = bf16[1024,512]{1,0:T(8,128)(2,1)} fusion(bf16[1024,2048]{1,0:T(8,128)(2,1)} %param.6, bf16[2048,512]{1,0:T(8,128)(2,1)} %param.7), kind=kOutput, calls=%fused_computation.16 | convolution fusion | flops 2148007936 | bytes 7340032 | tf_op jit(solution)/shard_map/dot_general | solution.py:28
  28.1 3.9 %collective-permute-done = bf16[256,1024]{1,0:T(8,128)(2,1)S(1)} collective-permute-done((bf16[256,1024]{1,0:T(8,128)(2,1)S(1)}, bf16[256,1024]{1,0:T(8,128)(2,1)S(1)}, u32[]{:S(2)}, u32[]{:S(2)}) %collective-permute-start) | collective-permute-done | bytes 524320 | tf_op jit(solution)/shard_map/ppermute | solution.py:24
  32.0 0.8 fusion.22
  32.8 13.5 %shard_map.117 = (bf16[1024,256]{1,0:T(8,128)(2,1)}, bf16[1024,256]{1,0:T(8,128)(2,1)}, bf16[1024,256]{1,0:T(8,128)(2,1)}, bf16[256,256]{1,0:T(8,128)(2,1)}, bf1...) custom-call(s32[1]{0:T(128)} %bitcast.first_ref, ...), custom_call_target="tpu_custom_call" | custom-call | flops 2415919104 | bytes 5242880 | tf_op jit(solution)/shard_map/pallas_call | solution.py:102
  46.3 1.0 pad_maximum_fusion.4
  47.4 1.3 collective-permute-start.1
  48.7 8.5 %collective-permute-done.1 = bf16[256,512]{1,0:T(8,128)(2,1)S(1)} collective-permute-done((bf16[256,512]{1,0:T(8,128)(2,1)S(1)}, bf16[256,512]{1,0:T(8,128)(2,1)S(1)}, u32[]{:S(2)}, u32[]{:S(2)}) %collective-permute-start.1) | collective-permute-done | bytes 262176 | tf_op jit(solution)/shard_map/ppermute | solution.py:24
  57.2 0.1 convert_element_type.51
  57.3 1.8 fusion.18
  59.1 7.6 %fusion = bf16[2048,768]{0,1:T(8,128)(2,1)} fusion(bf16[1024,2048]{1,0:T(8,128)(2,1)} %param.6, bf16[1024,256]{1,0:T(8,128)(2,1)} %get-tuple-element.46, bf16[1024,256]{1,0:T(8,128)(2,1)} %get-tuple-element.47, bf16[1024,256]{1,0:T(8,128)(2,1)S(1)} %copy-done.1), kind=kOutput, calls=%fused_computation.2 | convolution fusion | flops 3227516928 | bytes 8912896 | tf_op jit(solution)/shard_map/td,tc->dc/dot_general | solution.py:147
  66.7 0.2 reduce-scatter.5.cloned.1.call-start
  66.9 13.6 %shard_map.118 = (bf16[1024,256]{1,0:T(8,128)(2,1)}, bf16[1024,256]{1,0:T(8,128)(2,1)}, bf16[1024,256]{1,0:T(8,128)(2,1)}, bf16[256,256]{1,0:T(8,128)(2,1)}, bf1...) custom-call(s32[1]{0:T(128)} %bitcast.first_ref, ...), custom_call_target="tpu_custom_call" | custom-call | flops 2415919104 | bytes 5242880 | tf_op jit(solution)/shard_map/pallas_call | solution.py:102
  80.5 1.0 pad_maximum_fusion.5
  81.6 1.3 collective-permute-start.2
  82.9 8.3 %collective-permute-done.2 = bf16[256,512]{1,0:T(8,128)(2,1)S(1)} collective-permute-done((bf16[256,512]{1,0:T(8,128)(2,1)S(1)}, bf16[256,512]{1,0:T(8,128)(2,1)S(1)}, u32[]{:S(2)}, u32[]{:S(2)}) %collective-permute-start.2) | collective-permute-done | bytes 262176 | tf_op jit(solution)/shard_map/ppermute | solution.py:24
  91.2 0.1 convert_element_type.53
  91.3 1.8 fusion.19
  93.1 7.7 %fusion.1 = bf16[2048,768]{0,1:T(8,128)(2,1)} fusion(bf16[1024,2048]{1,0:T(8,128)(2,1)} %param.6, bf16[1024,256]{1,0:T(8,128)(2,1)} %get-tuple-element.48, bf16[1024,256]{1,0:T(8,128)(2,1)} %get-tuple-element.49, bf16[1024,256]{1,0:T(8,128)(2,1)S(1)} %copy-done.2), kind=kOutput, calls=%fused_computation.3 | convolution fusion | flops 3227516928 | bytes 8912896 | tf_op jit(solution)/shard_map/td,tc->dc/dot_general | solution.py:147
  100.9 0.6 copy-done.10
  101.5 31.4 %psum.7 = f32[4,512]{1,0:T(4,128)S(1)} all-reduce(f32[4,512]{1,0:T(4,128)S(1)} %bitcast.20), channel_id=1, replica_groups=mesh['sp'=8,'tp'=4] {'sp'}, use_global_device_ids=true, to_apply=%region_2.0 | all-reduce | flops 2048 | bytes 16384 | tf_op jit(solution)/shard_map/psum | solution.py:157
  133.0 0.1 slice.100
  133.1 0.1 slice_reduce_fusion.1
  133.2 0.1 slice_reduce_fusion
  133.3 0.1 copy.15
  133.4 0.2 reverse
  133.6 0.1 slice.126
  133.7 1.1 pad_maximum_fusion
  134.7 0.7 pad_maximum_fusion.8
  135.4 0.1 copy-done.6
  135.5 1.5 pad_maximum_fusion.1
  137.0 11.2 %reduce-scatter.3.cloned.1.call-done = bf16[256,768]{0,1:T(8,128)(2,1)} async-done(((bf16[2048,768]{0,1:T(8,128)(2,1)}), bf16[256,768]{0,1:T(8,128)(2,1)}) %reduce-scatter.3.cloned.1.call-update) | async-done | bytes 393232 | tf_op jit(solution)/shard_map/reduce_scatter | solution.py:149
  148.2 1.1 fusion.23
  149.3 76.7 %reduce-scatter.5.cloned.1.call-done = bf16[256,768]{0,1:T(8,128)(2,1)} async-done(((bf16[2048,768]{0,1:T(8,128)(2,1)}), bf16[256,768]{0,1:T(8,128)(2,1)}) %reduce-scatter.5.cloned.1.call-update) | async-done | bytes 393232 | tf_op jit(solution)/shard_map/reduce_scatter | solution.py:149
  225.9 1.7 fusion.24
  227.7 1.0 copy.18
  228.7 1.0 maximum_convert_fusion
  229.7 1.0 copy.16
  230.7 1.0 copy.17
  (36 shorter events, 0.2 us)
Async XLA Ops:
  7.2 1.6 copy-start
  7.2 141.0 %reduce-scatter.3.cloned.1.call-start = ((), (), s32[]{:S(2)}) async-start(), calls=%async_computation.2 | async-start | bytes 3538944 | tf_op jit(solution)/shard_map/reduce_scatter | solution.py:149
  8.8 4.7 %copy-start.12 = (bf16[1024,2048]{1,0:T(8,128)(2,1)S(1)}, bf16[1024,2048]{1,0:T(8,128)(2,1)}, u32[]{:S(2)}) copy-start(bf16[1024,2048]{1,0:T(8,128)(2,1)} %param.6) | copy-start | bytes 12582916
  8.8 4.7 %copy-start.13 = (bf16[2048,512]{1,0:T(8,128)(2,1)S(1)}, bf16[2048,512]{1,0:T(8,128)(2,1)}, u32[]{:S(2)}) copy-start(bf16[2048,512]{1,0:T(8,128)(2,1)} %param.9) | copy-start | bytes 6291460
  13.4 2.4 %copy-start.7 = (bf16[1024,512]{1,0:T(8,128)(2,1)}, bf16[1024,512]{1,0:T(8,128)(2,1)S(1)}, u32[]{:S(2)}) copy-start(bf16[1024,512]{1,0:T(8,128)(2,1)S(1)} %convolution_convert_fusion.3.k_ref) | copy-start | bytes 3145732
  13.5 7.4 %copy-start.9 = (f32[4,257]{1,0:T(4,128)S(1)}, f32[4,257]{1,0:T(4,128)}, u32[]{:S(2)}) copy-start(f32[4,257]{1,0:T(4,128)} %param.10) | copy-start | bytes 12340
  15.8 5.0 %copy-start.8 = (bf16[1024,512]{1,0:T(8,128)(2,1)}, bf16[1024,512]{1,0:T(8,128)(2,1)S(1)}, u32[]{:S(2)}) copy-start(bf16[1024,512]{1,0:T(8,128)(2,1)S(1)} %convolution_convert_fusion.2.v_ref) | copy-start | bytes 3145732
  15.9 16.0 %collective-permute-start = (bf16[256,1024]{1,0:T(8,128)(2,1)S(1)}, bf16[256,1024]{1,0:T(8,128)(2,1)S(1)}, u32[]{:S(2)}, u32[]{:S(2)}) collective-permute-start(bf16[256,1024]{1,0:T(8,128)(2,1)S(1)} %pad_maximum_fusion.3), channel_id=1, source_target_pairs={{0,4},{4,8},{8,12},{12,16},{16,20},{20,24},{24,28},{1,5},{5,9},{9,... | collective-permute-start | bytes 1572872 | tf_op jit(solution)/shard_map/ppermute | solution.py:24
  46.3 12.8 %copy-start.1 = (bf16[1024,256]{1,0:T(8,128)(2,1)S(1)}, bf16[1024,256]{1,0:T(8,128)(2,1)}, u32[]{:S(2)}) copy-start(bf16[1024,256]{1,0:T(8,128)(2,1)} %get-tuple-element.23) | copy-start | bytes 1572868
  47.4 9.8 %collective-permute-start.1 = (bf16[256,512]{1,0:T(8,128)(2,1)S(1)}, bf16[256,512]{1,0:T(8,128)(2,1)S(1)}, u32[]{:S(2)}, u32[]{:S(2)}) collective-permute-start(bf16[256,512]{1,0:T(8,128)(2,1)S(1)} %pad_maximum_fusion.4), channel_id=1, source_target_pairs={{4,0},{8,4},{12,8},{16,12},{20,16},{24,20},{28,24},{5,1},{9,5},{13... | collective-permute-start | bytes 786440 | tf_op jit(solution)/shard_map/ppermute | solution.py:24
  66.7 159.2 %reduce-scatter.5.cloned.1.call-start = ((), (), s32[]{:S(2)}) async-start(), calls=%async_computation.3 | async-start | bytes 3538944 | tf_op jit(solution)/shard_map/reduce_scatter | solution.py:149
  80.5 12.6 %copy-start.2 = (bf16[1024,256]{1,0:T(8,128)(2,1)S(1)}, bf16[1024,256]{1,0:T(8,128)(2,1)}, u32[]{:S(2)}) copy-start(bf16[1024,256]{1,0:T(8,128)(2,1)} %get-tuple-element.24) | copy-start | bytes 1572868
  81.6 9.6 %collective-permute-start.2 = (bf16[256,512]{1,0:T(8,128)(2,1)S(1)}, bf16[256,512]{1,0:T(8,128)(2,1)S(1)}, u32[]{:S(2)}, u32[]{:S(2)}) collective-permute-start(bf16[256,512]{1,0:T(8,128)(2,1)S(1)} %pad_maximum_fusion.5), channel_id=1, source_target_pairs={{4,0},{8,4},{12,8},{16,12},{20,16},{24,20},{28,24},{5,1},{9,5},{13... | collective-permute-start | bytes 786440 | tf_op jit(solution)/shard_map/ppermute | solution.py:24
  100.8 0.7 copy-start.10
  100.8 0.7 copy-start.11
  133.6 1.8 copy-start.3
  133.6 1.8 copy-start.4
  133.6 1.8 copy-start.5
  133.6 1.9 copy-start.6
Sparse Core Ops, SparseCore 0:
  66.8 81.3 reduce-scatter.2
  151.8 74.0 reduce-scatter.4
